TPU v7x, 512 devices: a whole 4x4x16 slice. The times are simulated.
512 devices in a mesh: sp: 32 (over z, core), tp: 16 (over y, x).
Axes of the slice: x: 4, y: 4, z: 16, core: 2. Of those that a mesh axis runs over, the one named last changes fastest.
Arguments:
- u_val: bfloat16 [8192, 2048], P('sp', 'tp'), may hold values from -6 to 6
- u_gate: bfloat16 [8192, 2048], P('sp', 'tp'), may hold values from -9 to 9
- conv_weight: float32 [31, 2048], P(None, 'tp')
- conv_bias: float32 [2048], P('tp'), may hold values from -3 to 3
- ln_gain: float32 [2048], P('tp'), may hold values from 0.1 to 1.9
- ln_bias: float32 [2048], P('tp'), may hold values from -3 to 3
- proj_weight: bfloat16 [2048, 4096], P(None, 'tp'), may hold values from -0.125 to 0.125
- resid: bfloat16 [8192, 4096], P('sp', 'tp')
- norm_gain: float32 [4096], P('tp'), may hold values from 0.1 to 1.9
- route_ids: int32 [8192, 2], P('sp'), may hold values from 0 to 31, all different within a row; in each aligned block of 256 rows (0 to 255, 256 to 511, ...) at most 32 rows name the same one
- route_wts: float32 [8192, 2], P('sp'), may hold values from 0.3 to 1.5
- expert_gate: bfloat16 [32, 4096, 1024], P('sp', None, 'tp'), may hold values from -0.09375 to 0.09375
- expert_up: bfloat16 [32, 4096, 1024], P('sp', None, 'tp'), may hold values from -0.09375 to 0.09375
- expert_down: bfloat16 [32, 1024, 4096], P('sp', None, 'tp'), may hold values from -0.1875 to 0.1875
- shared_gate: bfloat16 [4096, 1024], P(None, 'tp'), may hold values from -0.09375 to 0.09375
- shared_up: bfloat16 [4096, 1024], P(None, 'tp'), may hold values from -0.09375 to 0.09375
- shared_down: bfloat16 [1024, 4096], P(None, 'tp'), may hold values from -0.1875 to 0.1875
Outputs:
- mixed: bfloat16 [8192, 4096], P('sp', 'tp')
Inputs may be any that keep to these rules, and one draw needn't show every extreme that they name: `route_ids`: each row names 2 different experts. In each aligned block of 256 rows (the rows of one index of sp) no expert is named by more than 32 rows, a bound that some expert reaches in some blocks.
All inputs are finite; a program needn't handle non-finite values.
Results may differ from a plain program's by a relative error of at most 0.012.
Values may be sent and summed in bfloat16 or wider, within the bound.
A program may use at most 64 MiB of HBM per device.

v0:
```python
import jax
import jax.numpy as jnp
from jax import lax
from jax.sharding import PartitionSpec as P

D = 4096
CONV = 2048
norm_eps = 1e-06


def shifted(block, axis, distance):
    devices = range(lax.axis_size(axis))
    route = [(i - distance, i) for i in devices if i - distance in devices]
    return lax.ppermute(block, axis, route)


def from_everyone(array, axis):
    size = lax.axis_size(axis)
    return lax.all_to_all(
        jnp.broadcast_to(array[None], (size, *array.shape)), axis, 0, 0, tiled=True
    )


def over_copies(array, axis):
    return from_everyone(array, axis).sum(axis=0)


def in_one(arrays, axis):
    ravelled, at, gathered = (jnp.concatenate([a.reshape(-1) for a in arrays]), 0, [])
    subtotal = over_copies(ravelled, axis)
    for a in arrays:
        gathered.append(subtotal[at : at + a.size].reshape(a.shape))
        at += a.size
    return tuple(gathered)


def laid_out(pieces, dim):
    dims = list(pieces.shape[1:])
    dims[dim] *= pieces.shape[0]
    return jnp.moveaxis(pieces, 0, dim).reshape(dims)


def gather_directly(array, axis, dim):
    return laid_out(from_everyone(array, axis), dim)


def rows_first(arrays, axis, dims):
    turned = [jnp.moveaxis(a, dim, 0) for a, dim in zip(arrays, dims)]
    widths = [t[0].size for t in turned]
    both = jnp.concatenate([t.reshape(-1, w) for t, w in zip(turned, widths)], axis=1)
    out = lax.all_gather(both, axis, axis=0, tiled=True)
    pieces = jnp.split(out, [sum(widths[:k]) for k in range(1, len(widths))], axis=1)
    return tuple(
        (
            jnp.moveaxis(b.reshape(-1, *t.shape[1:]), 0, dim)
            for b, t, dim in zip(pieces, turned, dims)
        )
    )


def shards(
    u_val,
    u_gate,
    conv_weight,
    conv_bias,
    ln_gain,
    ln_bias,
    proj_weight,
    resid,
    norm_gain,
    route_ids,
    route_wts,
    expert_gate,
    expert_up,
    expert_down,
    shared_gate,
    shared_up,
    shared_down,
):
    tok_rows = u_val.shape[0]
    sp_count = lax.axis_size("sp")
    tp_count = lax.axis_size("tp")
    kernel_width = conv_weight.shape[0]
    gated = (u_val.astype(jnp.float32) * jax.nn.sigmoid(u_gate.astype(jnp.float32))).astype(
        jnp.bfloat16
    )
    rim_rows = shifted(gated[tok_rows - (kernel_width - 1) :], "sp", 1)
    padded = lax.optimization_barrier(jnp.concatenate([rim_rows, gated], axis=0)).astype(
        jnp.float32
    )
    conv_sum = jnp.zeros((tok_rows, gated.shape[1]), jnp.float32) + conv_bias[None, :]
    for tap_index in range(kernel_width):
        conv_sum = (
            conv_sum + conv_weight[tap_index][None, :] * padded[tap_index : tap_index + tok_rows]
        )
    stat_sums = in_one((jnp.sum(conv_sum, axis=1), jnp.sum(conv_sum * conv_sum, axis=1)), "tp")
    channel_mean = stat_sums[0] / CONV
    channel_var = stat_sums[1] / CONV - channel_mean * channel_mean
    normed_conv = (conv_sum - channel_mean[:, None]) * lax.rsqrt(channel_var + norm_eps)[:, None]
    conv_out = jax.nn.silu(normed_conv * ln_gain + ln_bias).astype(jnp.bfloat16)
    projected = jnp.dot(
        gather_directly(conv_out, "tp", 1), proj_weight, preferred_element_type=jnp.float32
    )
    residual_mid = (resid.astype(jnp.float32) + projected).astype(jnp.bfloat16)
    residual_wide = residual_mid.astype(jnp.float32)
    square_sum = over_copies(jnp.sum(residual_wide * residual_wide, axis=1), "tp")
    normed_rows = (
        residual_wide * lax.rsqrt(square_sum / D + norm_eps)[:, None] * norm_gain
    ).astype(jnp.bfloat16)
    rows_full = gather_directly(normed_rows, "tp", 1)
    topk_count = route_ids.shape[1]
    capacity = 2 * tok_rows * topk_count // sp_count
    pair_ids = route_ids.reshape(-1)
    onehot = (pair_ids[:, None] == jnp.arange(sp_count, dtype=jnp.int32)[None, :]).astype(jnp.int32)
    before = jnp.cumsum(onehot, axis=0) - onehot
    position = jnp.sum(before * onehot, axis=1)
    pair_slot = pair_ids * capacity + position
    matches = (
        jnp.arange(sp_count * capacity, dtype=jnp.int32)[:, None] == pair_slot[None, :]
    ).astype(jnp.int32)
    pair_tok = jnp.arange(tok_rows * topk_count, dtype=jnp.int32) // topk_count
    filled = jnp.sum(matches, axis=1)
    slot_tok = jnp.sum(matches * pair_tok[None, :], axis=1) + (1 - filled) * tok_rows
    rows_ext = jnp.concatenate(
        [rows_full, jnp.zeros((1, rows_full.shape[1]), jnp.bfloat16)], axis=0
    )
    part_slots = capacity // tp_count
    tp_index = lax.axis_index("tp")
    local_slots = lax.dynamic_slice_in_dim(
        slot_tok.reshape(sp_count, capacity), tp_index * part_slots, part_slots, 1
    )
    send_rows = jnp.take(rows_ext, local_slots.reshape(-1), axis=0).reshape(
        sp_count, part_slots, -1
    )
    received = lax.all_to_all(send_rows, "sp", split_axis=0, concat_axis=0, tiled=True)
    arrived = lax.all_gather(received, "tp", axis=1, tiled=True)
    slot_rows = arrived.reshape(sp_count * capacity, -1)
    gate_pre = jnp.dot(slot_rows, expert_gate[0], preferred_element_type=jnp.float32)
    up_proj = jnp.dot(slot_rows, expert_up[0], preferred_element_type=jnp.float32)
    hidden = (jax.nn.silu(gate_pre) * up_proj).astype(jnp.bfloat16)
    shared_pre = jnp.dot(rows_full, shared_gate, preferred_element_type=jnp.float32)
    shared_upper = jnp.dot(rows_full, shared_up, preferred_element_type=jnp.float32)
    shared_hidden = (jax.nn.silu(shared_pre) * shared_upper).astype(jnp.bfloat16)
    out_cols = expert_down.shape[2]
    pieces = rows_first((hidden, shared_hidden), "tp", (1, 1))
    routed_rows = expert_down[0]
    routed_out = jnp.dot(pieces[0], routed_rows, preferred_element_type=jnp.float32)
    shared_out = jnp.dot(pieces[1], shared_down, preferred_element_type=jnp.float32)
    expert_rows = routed_out.astype(jnp.bfloat16).reshape(sp_count, capacity, out_cols)
    returned_rows = lax.all_to_all(expert_rows, "sp", split_axis=0, concat_axis=0, tiled=True)
    returned_flat = returned_rows.reshape(sp_count * capacity, out_cols)
    picked = (
        jnp.take(returned_flat, pair_slot, axis=0)
        .astype(jnp.float32)
        .reshape(tok_rows, topk_count, out_cols)
    )
    routed = jnp.sum(picked * route_wts[:, :, None], axis=1)
    return (residual_wide + shared_out + routed).astype(jnp.bfloat16)


def solution(mesh):
    in_specs = (
        P("sp", "tp"),
        P("sp", "tp"),
        P(None, "tp"),
        P("tp"),
        P("tp"),
        P("tp"),
        P(None, "tp"),
        P("sp", "tp"),
        P("tp"),
        P("sp", None),
        P("sp", None),
        P("sp", None, "tp"),
        P("sp", None, "tp"),
        P("sp", None, "tp"),
        P(None, "tp"),
        P(None, "tp"),
        P(None, "tp"),
    )
    out_specs = P("sp", "tp")
    return jax.shard_map(shards, mesh=mesh, in_specs=in_specs, out_specs=out_specs, check_vma=False)
```

profile of v0, /device:TPU:1, one launch (start us, length us, event | category | flops | bytes accessed | tf_op | source)
XLA Modules:
  0.0 380.0 jit_solution(2414357554840305814)
XLA Ops:
  6.5 1.0 multiply_convert_fusion.2
  7.6 4.9 %collective-permute-start = (bf16[30,128]{1,0:T(8,128)(2,1)S(1)}, bf16[30,128]{1,0:T(8,128)(2,1)S(1)}, u32[]{:S(2)}, u32[]{:S(2)}) collective-permute-start(bf16[30,128]{1,0:T(8,128)(2,1)S(1)} %slice.272), channel_id=1, source_target_pairs={{0,16},{16,32},{32,48},{48,64},{64,80},{80,96},{96,112},{112,128},... | collective-permute-start | bytes 23048 | tf_op jit(solution)/shard_map/ppermute | solution.py:14
  12.5 1.0 slice_bitcast_fusion.30
  13.5 1.0 slice_bitcast_fusion.29
  14.5 1.9 collective-permute-done
  16.4 1.3 fusion.56
  17.7 11.3 %all_to_all.32 = f32[16,1,512]{2,1,0:T(1,128)S(1)} all-to-all(f32[16,1,512]{2,1,0:T(1,128)S(1)} %broadcast_in_dim.22), channel_id=1, replica_groups=mesh['sp'=32,'tp'=16] {'tp'}, dimensions={0} | all-to-all | bytes 65536 | tf_op jit(solution)/shard_map/all_to_all | solution.py:19
  29.1 0.2 multiply_convert_fusion.1
  29.4 1.1 broadcast_in_dim.23
  30.5 3.8 all-to-all-start.1
  34.4 16.9 %all-to-all-done.1 = bf16[16,256,128]{1,2,0:T(8,128)(2,1)S(1)} async-done(((bf16[16,256,128]{1,2,0:T(8,128)(2,1)}), bf16[16,256,128]{1,2,0:T(8,128)(2,1)S(1)}, u32[]{:S(2)}, u32[]{:S(2)}) %all-to-all-start.1) | async-done | bytes 1048608 | tf_op jit(solution)/shard_map/all_to_all | solution.py:19
  51.3 0.5 multiply_reduce_fusion.1
  51.9 10.3 %all_to_all.33 = f32[16,1,256]{2,1,0:T(1,128)S(1)} all-to-all(f32[16,1,256]{2,1,0:T(1,128)S(1)} %broadcast_in_dim.25), channel_id=1, replica_groups=mesh['sp'=32,'tp'=16] {'tp'}, dimensions={0} | all-to-all | bytes 32768 | tf_op jit(solution)/shard_map/all_to_all | solution.py:19
  62.4 1.6 broadcast_in_dim.26
  64.0 3.8 %all-to-all-start.3 = ((bf16[16,256,256]{2,1,0:T(8,128)(2,1)}), bf16[16,256,256]{2,1,0:T(8,128)(2,1)S(1)}, u32[]{:S(2)}, u32[]{:S(2)}) async-start(bf16[16,256,256]{2,1,0:T(8,128)(2,1)} %broadcast_in_dim.26), calls=%async_computation.3 | async-start | bytes 4194304 | tf_op jit(solution)/shard_map/all_to_all | solution.py:19
  68.0 0.1 reshape.176
  68.2 0.1 eq.40
  68.3 1.2 reduce-window.6
  69.5 0.2 slice_reduce_fusion
  69.9 0.6 convert_reduce_fusion
  70.8 24.7 %all-to-all-done.3 = bf16[16,256,256]{2,1,0:T(8,128)(2,1)S(1)} async-done(((bf16[16,256,256]{2,1,0:T(8,128)(2,1)}), bf16[16,256,256]{2,1,0:T(8,128)(2,1)S(1)}, u32[]{:S(2)}, u32[]{:S(2)}) %all-to-all-start.3) | async-done | bytes 2097184 | tf_op jit(solution)/shard_map/all_to_all | solution.py:19
  95.5 1.3 copy-done.2
  96.8 1.8 copy.131
  98.7 1.6 concatenate.14
  100.2 4.1 %gather_fusion = bf16[64,4096]{1,0:T(8,128)(2,1)} fusion(bf16[257,4096]{1,0:T(8,128)(2,1)} %concatenate.14, s32[1024]{0:T(1024)S(1)} %pad_clamp_fusion.1), kind=kCustom, calls=%fused_computation | custom fusion | bytes 1048832 | tf_op jit(solution)/shard_map/jit(_take)/gather | solution.py:132
  104.3 2.2 gather.13
  106.4 1.6 broadcast_select_fusion
  108.1 52.7 %all_to_all.34 = bf16[32,2,4096]{2,1,0:T(2,128)(2,1)S(1)} all-to-all(bf16[32,2,4096]{2,1,0:T(2,128)(2,1)S(1)} %broadcast_select_fusion), channel_id=1, replica_groups=mesh['sp'=32,'tp'=16] {'sp'}, dimensions={0} | all-to-all | bytes 1048576 | tf_op jit(solution)/shard_map/all_to_all | solution.py:135
  160.8 1.1 copy.116
  162.0 0.2 all-gather.5.cloned.1.call-start
  162.2 1.9 convolution_bitcast_fusion.3
  164.1 0.8 fusion.12
  164.8 70.4 %all-gather.3.cloned.1.call-done = bf16[32,32,4096]{2,0,1:T(8,128)(2,1)} async-done(((bf16[32,2,4096]{2,0,1:T(8,128)(2,1)}), bf16[32,32,4096]{2,0,1:T(8,128)(2,1)}) %all-gather.3.cloned.1.call-update) | async-done | bytes 8388624 | tf_op jit(solution)/shard_map/all_gather | solution.py:136
  235.3 11.2 %copy.117 = bf16[32,32,4096]{2,1,0:T(8,128)(2,1)} copy(bf16[32,32,4096]{2,0,1:T(8,128)(2,1)} %all-gather.3.cloned.1.call-done) | data formatting | bytes 16777216 | tf_op jit(solution)/shard_map/all_gather | solution.py:136
  246.5 6.2 %convolution_bitcast_fusion.1 = f32[64,1024]{1,0:T(8,128)S(1)} fusion(bf16[1024,4096]{1,0:T(8,128)(2,1)} %bitcast.128, bf16[1,4096,64]{1,2,0:T(8,128)(2,1)S(1)} %copy-done.3), kind=kOutput, calls=%fused_computation.9 | convolution fusion | flops 536870912 | bytes 9175040 | tf_op jit(solution)/shard_map/dot_general | solution.py:138
  252.7 2.7 fusion.9
  255.3 0.7 pad_maximum_fusion
  256.1 60.2 %all-gather.5.cloned.1.call-done = bf16[1024,1280]{1,0:T(8,128)(2,1)} async-done(((bf16[64,1280]{1,0:T(8,128)(2,1)}), bf16[1024,1280]{1,0:T(8,128)(2,1)}) %all-gather.5.cloned.1.call-update) | async-done | bytes 2621456 | tf_op jit(solution)/shard_map/all_gather | solution.py:51
  316.3 3.2 fusion.2
  319.5 14.3 %all-to-all-start.5 = ((bf16[32,32,256]{2,1,0:T(8,128)(2,1)}), bf16[32,32,256]{2,1,0:T(8,128)(2,1)S(1)}, u32[]{:S(2)}, u32[]{:S(2)}) async-start(bf16[32,32,256]{2,1,0:T(8,128)(2,1)} %bitcast.44), calls=%async_computation.5 | async-start | bytes 1048576 | tf_op jit(solution)/shard_map/all_to_all | solution.py:150
  333.8 0.1 reduce_sum.93
  334.1 0.1 mul.553
  334.3 0.2 copy.120
  334.7 32.6 %all-to-all-done.5 = bf16[32,32,256]{2,1,0:T(8,128)(2,1)S(1)} async-done(((bf16[32,32,256]{2,1,0:T(8,128)(2,1)}), bf16[32,32,256]{2,1,0:T(8,128)(2,1)S(1)}, u32[]{:S(2)}, u32[]{:S(2)}) %all-to-all-start.5) | async-done | bytes 524320 | tf_op jit(solution)/shard_map/all_to_all | solution.py:150
  367.3 1.9 gather_fusion.1
  369.4 1.5 multiply_reduce_fusion
  371.0 1.4 fusion.10
  372.4 0.8 copy.124
  (65 shorter events, 1.9 us)
Async XLA Ops:
  6.5 44.8 %copy-start = (bf16[2048,256]{1,0:T(8,128)(2,1)S(1)}, bf16[2048,256]{1,0:T(8,128)(2,1)}, u32[]{:S(2)}) copy-start(bf16[2048,256]{1,0:T(8,128)(2,1)} %param.23) | copy-start | bytes 3145732
  7.6 8.8 %collective-permute-start = (bf16[30,128]{1,0:T(8,128)(2,1)S(1)}, bf16[30,128]{1,0:T(8,128)(2,1)S(1)}, u32[]{:S(2)}, u32[]{:S(2)}) collective-permute-start(bf16[30,128]{1,0:T(8,128)(2,1)S(1)} %slice.272), channel_id=1, source_target_pairs={{0,16},{16,32},{32,48},{48,64},{64,80},{80,96},{96,112},{112,128},... | collective-permute-start | bytes 23048 | tf_op jit(solution)/shard_map/ppermute | solution.py:14
  16.4 12.7 %copy-start.10 = (f32[128]{0:T(128)S(1)}, f32[128]{0:T(128)}, u32[]{:S(2)}) copy-start(f32[128]{0:T(128)} %param.22) | copy-start | bytes 1540
  16.4 12.7 %copy-start.11 = (f32[128]{0:T(128)S(1)}, f32[128]{0:T(128)}, u32[]{:S(2)}) copy-start(f32[128]{0:T(128)} %param.21) | copy-start | bytes 1540
  17.7 16.6 %copy-start.6 = (bf16[256,256]{1,0:T(8,128)(2,1)S(1)}, bf16[256,256]{1,0:T(8,128)(2,1)}, u32[]{:S(2)}) copy-start(bf16[256,256]{1,0:T(8,128)(2,1)} %param.24) | copy-start | bytes 393220
  30.5 31.7 %copy-start.9 = (f32[256]{0:T(256)S(1)}, f32[256]{0:T(256)}, u32[]{:S(2)}) copy-start(f32[256]{0:T(256)} %param.25) | copy-start | bytes 3076
  30.5 20.8 %all-to-all-start.1 = ((bf16[16,256,128]{1,2,0:T(8,128)(2,1)}), bf16[16,256,128]{1,2,0:T(8,128)(2,1)S(1)}, u32[]{:S(2)}, u32[]{:S(2)}) async-start(bf16[16,256,128]{1,2,0:T(8,128)(2,1)} %broadcast_in_dim.23), calls=%async_computation.1 | async-start | bytes 2097152 | tf_op jit(solution)/shard_map/all_to_all | solution.py:19
  64.0 3.9 %copy-start.7 = (s32[256,2]{0,1:T(2,128)S(1)}, s32[256,2]{0,1:T(2,128)}, u32[]{:S(2)}) copy-start(s32[256,2]{0,1:T(2,128)} %param.26) | copy-start | bytes 6148
  64.0 31.5 %all-to-all-start.3 = ((bf16[16,256,256]{2,1,0:T(8,128)(2,1)}), bf16[16,256,256]{2,1,0:T(8,128)(2,1)S(1)}, u32[]{:S(2)}, u32[]{:S(2)}) async-start(bf16[16,256,256]{2,1,0:T(8,128)(2,1)} %broadcast_in_dim.26), calls=%async_computation.3 | async-start | bytes 4194304 | tf_op jit(solution)/shard_map/all_to_all | solution.py:19
  67.8 167.5 %all-gather.3.cloned.1.call-start = ((), (), s32[]{:S(2)}) async-start(), calls=%async_computation.6 | async-start | bytes 8912896 | tf_op jit(solution)/shard_map/all_gather | solution.py:136
  95.5 1.4 copy-start.2
  162.0 154.3 %all-gather.5.cloned.1.call-start = ((), (), s32[]{:S(2)}) async-start(), calls=%async_computation.7 | async-start | bytes 2785280 | tf_op jit(solution)/shard_map/all_gather | solution.py:51
  162.2 1.9 copy-start.5
  164.8 81.6 %copy-start.3 = (bf16[1,4096,64]{1,2,0:T(8,128)(2,1)S(1)}, bf16[1,4096,64]{1,2,0:T(8,128)(2,1)}, u32[]{:S(2)}) copy-start(bf16[1,4096,64]{1,2,0:T(8,128)(2,1)} %param.28) | copy-start | bytes 1572868
  246.5 6.2 %copy-start.1 = (bf16[32,32,4096]{2,1,0:T(8,128)(2,1)S(1)}, bf16[32,32,4096]{2,1,0:T(8,128)(2,1)}, u32[]{:S(2)}) copy-start(bf16[32,32,4096]{2,1,0:T(8,128)(2,1)} %copy.117) | copy-start | bytes 25165828
  246.5 6.2 %copy-start.12 = (bf16[1,4096,64]{1,2,0:T(8,128)(2,1)S(1)}, bf16[1,4096,64]{1,2,0:T(8,128)(2,1)}, u32[]{:S(2)}) copy-start(bf16[1,4096,64]{1,2,0:T(8,128)(2,1)} %param.29) | copy-start | bytes 1572868
  252.7 63.6 %copy-start.13 = (bf16[1,1024,256]{2,1,0:T(8,128)(2,1)S(1)}, bf16[1,1024,256]{2,1,0:T(8,128)(2,1)}, u32[]{:S(2)}) copy-start(bf16[1,1024,256]{2,1,0:T(8,128)(2,1)} %param.30) | copy-start | bytes 1572868
  256.0 78.5 %copy-start.8 = (f32[256,2]{0,1:T(2,128)S(1)}, f32[256,2]{0,1:T(2,128)}, u32[]{:S(2)}) copy-start(f32[256,2]{0,1:T(2,128)} %param.27) | copy-start | bytes 6148
  319.5 47.8 %all-to-all-start.5 = ((bf16[32,32,256]{2,1,0:T(8,128)(2,1)}), bf16[32,32,256]{2,1,0:T(8,128)(2,1)S(1)}, u32[]{:S(2)}, u32[]{:S(2)}) async-start(bf16[32,32,256]{2,1,0:T(8,128)(2,1)} %bitcast.44), calls=%async_computation.5 | async-start | bytes 1048576 | tf_op jit(solution)/shard_map/all_to_all | solution.py:150
  334.5 36.5 %copy-start.4 = (bf16[1024,256]{1,0:T(8,128)(2,1)S(1)}, bf16[1024,256]{1,0:T(8,128)(2,1)}, u32[]{:S(2)}) copy-start(bf16[1024,256]{1,0:T(8,128)(2,1)} %param.33) | copy-start | bytes 1572868
Sparse Core Ops, SparseCore 0:
  162.1 73.1 all-gather.2
  256.2 60.0 all-gather.4
where the time goes:
time: 381 us; the launch traced here: 380 us
  waiting for transfers between devices  207 us (54%)
  blocking collectives  74.3 us (20%)
  local copies, waits for them, and re-layouts  32.9 us (9%)
  starting transfers between devices  27.1 us (7%)
  matrix products  16.6 us (4%)
  between operations  13.8 us (4%)
  other arithmetic  8.53 us (2%)
    all_gather x1, waiting for transfers between devices, shards(): arrived = lax.all_gather(received, 'tp', axis=1, tiled=True)  70.4 us
    all_gather x1, waiting for transfers between devices, rows_first(): out = lax.all_gather(both, axis, axis=0, tiled=True)  60.2 us
    all_to_all x1, blocking collectives, shards(): lax.all_to_all(send_rows, 'sp', split_axis=0, concat_axis=0, tiled=True)  52.7 us
    all_to_all x2, waiting for transfers between devices, from_everyone(): lax.all_to_all(jnp.broadcast_to(array[None], (size, *array.shape)), axis,...  41.6 us
    all_to_all x1, waiting for transfers between devices, shards(): lax.all_to_all(expert_rows, 'sp', split_axis=0, concat_axis=0, tiled=True)  32.6 us
    all_to_all x2, blocking collectives, from_everyone(): lax.all_to_all(jnp.broadcast_to(array[None], (size, *array.shape)), axis,...  21.6 us
    all_to_all x1, starting transfers between devices, shards(): lax.all_to_all(expert_rows, 'sp', split_axis=0, concat_axis=0, tiled=True)  14.3 us
    all_gather x1, local copies, waits for them, and re-layouts, shards(): arrived = lax.all_gather(received, 'tp', axis=1, tiled=True)  11.2 us
  transfers between devices with their start and end apart: 6, of which 6 were waited for; matrix products, arithmetic and copies ran while one was open for 2% of the time, Pallas kernels for 0%

commit v1 on v0

--- a/solution.py
+++ b/solution.py
@@ -2,6 +2,7 @@
 import jax.numpy as jnp
 from jax import lax
 from jax.sharding import PartitionSpec as P
+from jax.lax import axis_index, axis_size, ppermute
 
 D = 4096
 CONV = 2048
@@ -77,6 +78,29 @@
     shared_up,
     shared_down,
 ):
+
+    def state_lanes(x_local):
+        mid_arr, right_arr, clean = (axis_size("tp"), axis_index("tp"), x_local.shape[1])
+        pile = [(hop_no, (hop_no + 1) % mid_arr) for hop_no in range(mid_arr)]
+        series = [(hop_no, (hop_no - 1) % mid_arr) for hop_no in range(mid_arr)]
+        next_value = jnp.zeros(
+            (*x_local.shape[:1], mid_arr * clean, *x_local.shape[2:]), x_local.dtype
+        )
+        next_value = lax.dynamic_update_slice_in_dim(next_value, x_local, right_arr * clean, axis=1)
+        w_next = raw_out = x_local
+        lower = mid_arr // 2
+        for j0 in range(1, lower + 1):
+            w_next = ppermute(w_next, "tp", pile)
+            next_value = lax.dynamic_update_slice_in_dim(
+                next_value, w_next, (right_arr - j0) % mid_arr * clean, axis=1
+            )
+            if j0 < mid_arr - lower:
+                raw_out = ppermute(raw_out, "tp", series)
+                next_value = lax.dynamic_update_slice_in_dim(
+                    next_value, raw_out, (right_arr + j0) % mid_arr * clean, axis=1
+                )
+        return next_value
+
     tok_rows = u_val.shape[0]
     sp_count = lax.axis_size("sp")
     tp_count = lax.axis_size("tp")
@@ -133,7 +157,7 @@
         sp_count, part_slots, -1
     )
     received = lax.all_to_all(send_rows, "sp", split_axis=0, concat_axis=0, tiled=True)
-    arrived = lax.all_gather(received, "tp", axis=1, tiled=True)
+    arrived = state_lanes(received)
     slot_rows = arrived.reshape(sp_count * capacity, -1)
     gate_pre = jnp.dot(slot_rows, expert_gate[0], preferred_element_type=jnp.float32)
     up_proj = jnp.dot(slot_rows, expert_up[0], preferred_element_type=jnp.float32)

time: 381 us -> 416 us (1.092)
  starting transfers between devices: 27.1 us -> 109 us
  blocking collectives: 74.3 us -> 21.4 us
    all_gather x1 -> x0, waiting for transfers between devices: 70.4 us -> none  [shards(): arrived = lax.all_gather(received, 'tp', axis=1, tiled=True)]
    ppermute x0 -> x15, starting transfers between devices: none -> 62.4 us  [the longest x7 47 us: state_lanes(): raw_out = ppermute(raw_out, 'tp', series)]
    all_to_all x1 -> x0, blocking collectives: 52.7 us -> none  [shards(): lax.all_to_all(send_rows, 'sp', split_axis=0, concat_axis=0, tiled=True)]
    ppermute x0 -> x15, waiting for transfers between devices: none -> 44.4 us  [the longest x8 44.4 us: state_lanes(): w_next = ppermute(w_next, 'tp', pile)]
    all_to_all x0 -> x1, waiting for transfers between devices: none -> 31.4 us  [shards(): lax.all_to_all(send_rows, 'sp', split_axis=0, concat_axis=0, tiled=True)]
    all_to_all x0 -> x1, starting transfers between devices: none -> 19.5 us  [shards(): lax.all_to_all(send_rows, 'sp', split_axis=0, concat_axis=0, tiled=True)]
    dynamic_update_slice x0 -> x16, local copies, waits for them, and re-layouts: none -> 13.7 us  [the longest x8 6.3 us: state_lanes(): lax.dynamic_update_slice_in_dim(next_value, w_next, (right_arr - j0) % mi...]
    all_gather x1 -> x0, local copies, waits for them, and re-layouts: 11.2 us -> none  [shards(): arrived = lax.all_gather(received, 'tp', axis=1, tiled=True)]
  transfers between devices with their start and end apart: 6 -> 21, of which waited for: 6 -> 14; matrix products, arithmetic and copies ran while one was open for 2% -> 6% of each run, Pallas kernels for 0% -> 0%
where the time goes in v1:
time: 416 us; the launch traced here: 415 us
  waiting for transfers between devices  211 us (51%)
  starting transfers between devices  109 us (26%)
  local copies, waits for them, and re-layouts  35.3 us (8%)
  blocking collectives  21.4 us (5%)
  between operations  14.4 us (3%)
  matrix products  14 us (3%)
  other arithmetic  9.99 us (2%)
    all_gather x1, waiting for transfers between devices, rows_first(): out = lax.all_gather(both, axis, axis=0, tiled=True)  59.3 us
    ppermute x7, starting transfers between devices, state_lanes(): raw_out = ppermute(raw_out, 'tp', series)  47 us
    ppermute x8, waiting for transfers between devices, state_lanes(): w_next = ppermute(w_next, 'tp', pile)  44.4 us
    all_to_all x2, waiting for transfers between devices, from_everyone(): lax.all_to_all(jnp.broadcast_to(array[None], (size, *array.shape)), axis,...  41.6 us
    all_to_all x1, waiting for transfers between devices, shards(): lax.all_to_all(expert_rows, 'sp', split_axis=0, concat_axis=0, tiled=True)  32.6 us
    all_to_all x1, waiting for transfers between devices, shards(): lax.all_to_all(send_rows, 'sp', split_axis=0, concat_axis=0, tiled=True)  31.4 us
    all_to_all x2, blocking collectives, from_everyone(): lax.all_to_all(jnp.broadcast_to(array[None], (size, *array.shape)), axis,...  21.4 us
    all_to_all x1, starting transfers between devices, shards(): lax.all_to_all(send_rows, 'sp', split_axis=0, concat_axis=0, tiled=True)  19.5 us
  transfers between devices with their start and end apart: 21, of which 14 were waited for; matrix products, arithmetic and copies ran while one was open for 6% of the time, Pallas kernels for 0%

profile of v1, /device:TPU:1, one launch (start us, length us, event | category | flops | bytes accessed | tf_op | source)
XLA Modules:
  0.0 414.9 jit_solution(12258645355059588128)
XLA Ops:
  7.6 4.9 %collective-permute-start = (bf16[30,128]{1,0:T(8,128)(2,1)S(1)}, bf16[30,128]{1,0:T(8,128)(2,1)S(1)}, u32[]{:S(2)}, u32[]{:S(2)}) collective-permute-start(bf16[30,128]{1,0:T(8,128)(2,1)S(1)} %slice.272), channel_id=1, source_target_pairs={{0,16},{16,32},{32,48},{48,64},{64,80},{80,96},{96,112},{112,128},... | collective-permute-start | bytes 23048 | tf_op jit(solution)/shard_map/ppermute | solution.py:15
  14.5 1.9 collective-permute-done
  17.7 11.1 %all_to_all.32 = f32[16,1,512]{2,1,0:T(1,128)S(1)} all-to-all(f32[16,1,512]{2,1,0:T(1,128)S(1)} %broadcast_in_dim.24), channel_id=1, replica_groups=mesh['sp'=32,'tp'=16] {'tp'}, dimensions={0} | all-to-all | bytes 65536 | tf_op jit(solution)/shard_map/all_to_all | solution.py:20
  30.9 3.7 all-to-all-start.1
  34.7 16.9 %all-to-all-done.1 = bf16[16,256,128]{1,2,0:T(8,128)(2,1)S(1)} async-done(((bf16[16,256,128]{1,2,0:T(8,128)(2,1)}), bf16[16,256,128]{1,2,0:T(8,128)(2,1)S(1)}, u32[]{:S(2)}, u32[]{:S(2)}) %all-to-all-start.1) | async-done | bytes 1048608 | tf_op jit(solution)/shard_map/all_to_all | solution.py:20
  52.2 10.3 %all_to_all.33 = f32[16,1,256]{2,1,0:T(1,128)S(1)} all-to-all(f32[16,1,256]{2,1,0:T(1,128)S(1)} %broadcast_in_dim.28), channel_id=1, replica_groups=mesh['sp'=32,'tp'=16] {'tp'}, dimensions={0} | all-to-all | bytes 32768 | tf_op jit(solution)/shard_map/all_to_all | solution.py:20
  64.3 3.7 all-to-all-start.3
  71.0 24.7 %all-to-all-done.3 = bf16[16,256,256]{2,1,0:T(8,128)(2,1)S(1)} async-done(((bf16[16,256,256]{2,1,0:T(8,128)(2,1)}), bf16[16,256,256]{2,1,0:T(8,128)(2,1)S(1)}, u32[]{:S(2)}, u32[]{:S(2)}) %all-to-all-start.3) | async-done | bytes 2097184 | tf_op jit(solution)/shard_map/all_to_all | solution.py:20
  97.0 1.8 copy.94
  98.9 1.6 concatenate.14
  100.5 4.1 gather_fusion
  104.5 2.2 gather.13
  106.7 2.4 broadcast_select_fusion
  109.1 19.5 %all-to-all-start.4 = ((bf16[32,2,4096]{2,1,0:T(2,128)(2,1)}), bf16[32,2,4096]{2,1,0:T(2,128)(2,1)}, u32[]{:S(2)}, u32[]{:S(2)}) async-start(bf16[32,2,4096]{2,1,0:T(2,128)(2,1)} %broadcast_select_fusion), calls=%async_computation.4 | async-start | bytes 1048576 | tf_op jit(solution)/shard_map/all_to_all | solution.py:159
  128.9 1.8 convolution_bitcast_fusion.3
  130.7 31.4 %all-to-all-done.4 = bf16[32,2,4096]{2,1,0:T(2,128)(2,1)} async-done(((bf16[32,2,4096]{2,1,0:T(2,128)(2,1)}), bf16[32,2,4096]{2,1,0:T(2,128)(2,1)}, u32[]{:S(2)}, u32[]{:S(2)}) %all-to-all-start.4) | async-done | bytes 524320 | tf_op jit(solution)/shard_map/all_to_all | solution.py:159
  162.1 1.9 collective-permute-start.1
  164.1 6.7 %collective-permute-start.2 = (bf16[32,2,4096]{2,1,0:T(2,128)(2,1)}, bf16[32,2,4096]{2,1,0:T(2,128)(2,1)S(1)}, u32[]{:S(2)}, u32[]{:S(2)}) collective-permute-start(bf16[32,2,4096]{2,1,0:T(2,128)(2,1)} %all-to-all-done.4), channel_id=1, source_target_pairs={{0,15},{1,0},{2,1},{3,2},{4,3},{5,4},{6,5},{7,6},{8,7},{9,8},{10,9... | collective-permute-start | bytes 1572872 | tf_op jit(solution)/shard_map/ppermute | solution.py:98
  170.7 1.8 fusion.10
  173.6 1.9 constant_dynamic-update-slice_fusion.15
  175.5 5.0 %collective-permute-done.1 = bf16[32,2,4096]{2,1,0:T(2,128)(2,1)S(1)} collective-permute-done((bf16[32,2,4096]{2,1,0:T(2,128)(2,1)}, bf16[32,2,4096]{2,1,0:T(2,128)(2,1)S(1)}, u32[]{:S(2)}, u32[]{:S(2)}) %collective-permute-start.1) | collective-permute-done | bytes 524320 | tf_op jit(solution)/shard_map/ppermute | solution.py:93
  180.5 1.9 collective-permute-start.3
  182.5 6.9 %collective-permute-start.4 = (bf16[32,2,4096]{2,1,0:T(2,128)(2,1)S(1)}, bf16[32,2,4096]{2,1,0:T(2,128)(2,1)S(1)}, u32[]{:S(2)}, u32[]{:S(2)}) collective-permute-start(bf16[32,2,4096]{2,1,0:T(2,128)(2,1)S(1)} %collective-permute-done.2), channel_id=1, source_target_pairs={{0,15},{1,0},{2,1},{3,2},{4,3},{5,4},{6,5},{7,6},{8,7},{9,8},{10,9... | collective-permute-start | bytes 1572872 | tf_op jit(solution)/shard_map/ppermute | solution.py:98
  190.9 6.9 %collective-permute-done.3 = bf16[32,2,4096]{2,1,0:T(2,128)(2,1)S(1)} collective-permute-done((bf16[32,2,4096]{2,1,0:T(2,128)(2,1)S(1)}, bf16[32,2,4096]{2,1,0:T(2,128)(2,1)S(1)}, u32[]{:S(2)}, u32[]{:S(2)}) %collective-permute-start.3) | collective-permute-done | bytes 524320 | tf_op jit(solution)/shard_map/ppermute | solution.py:93
  197.9 1.9 collective-permute-start.5
  199.8 6.7 %collective-permute-start.6 = (bf16[32,2,4096]{2,1,0:T(2,128)(2,1)S(1)}, bf16[32,2,4096]{2,1,0:T(2,128)(2,1)S(1)}, u32[]{:S(2)}, u32[]{:S(2)}) collective-permute-start(bf16[32,2,4096]{2,1,0:T(2,128)(2,1)S(1)} %collective-permute-done.4), channel_id=1, source_target_pairs={{0,15},{1,0},{2,1},{3,2},{4,3},{5,4},{6,5},{7,6},{8,7},{9,8},{10,9... | collective-permute-start | bytes 1572872 | tf_op jit(solution)/shard_map/ppermute | solution.py:98
  208.1 6.3 %collective-permute-done.5 = bf16[32,2,4096]{2,1,0:T(2,128)(2,1)S(1)} collective-permute-done((bf16[32,2,4096]{2,1,0:T(2,128)(2,1)S(1)}, bf16[32,2,4096]{2,1,0:T(2,128)(2,1)S(1)}, u32[]{:S(2)}, u32[]{:S(2)}) %collective-permute-start.5) | collective-permute-done | bytes 524320 | tf_op jit(solution)/shard_map/ppermute | solution.py:93
  214.3 1.9 collective-permute-start.7
  216.3 6.7 %collective-permute-start.8 = (bf16[32,2,4096]{2,1,0:T(2,128)(2,1)S(1)}, bf16[32,2,4096]{2,1,0:T(2,128)(2,1)S(1)}, u32[]{:S(2)}, u32[]{:S(2)}) collective-permute-start(bf16[32,2,4096]{2,1,0:T(2,128)(2,1)S(1)} %collective-permute-done.6), channel_id=1, source_target_pairs={{0,15},{1,0},{2,1},{3,2},{4,3},{5,4},{6,5},{7,6},{8,7},{9,8},{10,9... | collective-permute-start | bytes 1572872 | tf_op jit(solution)/shard_map/ppermute | solution.py:98
  224.5 5.4 %collective-permute-done.7 = bf16[32,2,4096]{2,1,0:T(2,128)(2,1)S(1)} collective-permute-done((bf16[32,2,4096]{2,1,0:T(2,128)(2,1)S(1)}, bf16[32,2,4096]{2,1,0:T(2,128)(2,1)S(1)}, u32[]{:S(2)}, u32[]{:S(2)}) %collective-permute-start.7) | collective-permute-done | bytes 524320 | tf_op jit(solution)/shard_map/ppermute | solution.py:93
  229.9 1.9 collective-permute-start.9
  231.9 6.7 %collective-permute-start.10 = (bf16[32,2,4096]{2,1,0:T(2,128)(2,1)S(1)}, bf16[32,2,4096]{2,1,0:T(2,128)(2,1)S(1)}, u32[]{:S(2)}, u32[]{:S(2)}) collective-permute-start(bf16[32,2,4096]{2,1,0:T(2,128)(2,1)S(1)} %collective-permute-done.8), channel_id=1, source_target_pairs={{0,15},{1,0},{2,1},{3,2},{4,3},{5,4},{6,5},{7,6},{8,7},{9,8},{10,9... | collective-permute-start | bytes 1572872 | tf_op jit(solution)/shard_map/ppermute | solution.py:98
  240.2 4.5 %collective-permute-done.9 = bf16[32,2,4096]{2,1,0:T(2,128)(2,1)S(1)} collective-permute-done((bf16[32,2,4096]{2,1,0:T(2,128)(2,1)S(1)}, bf16[32,2,4096]{2,1,0:T(2,128)(2,1)S(1)}, u32[]{:S(2)}, u32[]{:S(2)}) %collective-permute-start.9) | collective-permute-done | bytes 524320 | tf_op jit(solution)/shard_map/ppermute | solution.py:93
  244.7 1.9 collective-permute-start.11
  246.6 6.7 %collective-permute-start.12 = (bf16[32,2,4096]{2,1,0:T(2,128)(2,1)S(1)}, bf16[32,2,4096]{2,1,0:T(2,128)(2,1)S(1)}, u32[]{:S(2)}, u32[]{:S(2)}) collective-permute-start(bf16[32,2,4096]{2,1,0:T(2,128)(2,1)S(1)} %collective-permute-done.10), channel_id=1, source_target_pairs={{0,15},{1,0},{2,1},{3,2},{4,3},{5,4},{6,5},{7,6},{8,7},{9,8},{10,9... | collective-permute-start | bytes 1572872 | tf_op jit(solution)/shard_map/ppermute | solution.py:98
  254.9 3.7 collective-permute-done.11
  258.6 1.9 collective-permute-start.13
  260.5 6.7 %collective-permute-start.14 = (bf16[32,2,4096]{2,1,0:T(2,128)(2,1)S(1)}, bf16[32,2,4096]{2,1,0:T(2,128)(2,1)S(1)}, u32[]{:S(2)}, u32[]{:S(2)}) collective-permute-start(bf16[32,2,4096]{2,1,0:T(2,128)(2,1)S(1)} %collective-permute-done.12), channel_id=1, source_target_pairs={{0,15},{1,0},{2,1},{3,2},{4,3},{5,4},{6,5},{7,6},{8,7},{9,8},{10,9... | collective-permute-start | bytes 1572872 | tf_op jit(solution)/shard_map/ppermute | solution.py:98
  268.8 3.0 collective-permute-done.13
  271.8 2.1 collective-permute-start.15
  275.6 9.5 %collective-permute-done.15 = bf16[32,2,4096]{2,1,0:T(2,128)(2,1)S(1)} collective-permute-done((bf16[32,2,4096]{2,1,0:T(2,128)(2,1)S(1)}, bf16[32,2,4096]{2,1,0:T(2,128)(2,1)S(1)}, u32[]{:S(2)}, u32[]{:S(2)}) %collective-permute-start.15) | collective-permute-done | bytes 524320 | tf_op jit(solution)/shard_map/ppermute | solution.py:93
  285.9 2.7 convolution_bitcast_fusion.1
  288.6 2.7 multiply_convert_fusion
  292.0 59.3 %all-gather.2.cloned.1.call-done = bf16[1024,1280]{1,0:T(8,128)(2,1)} async-done(((bf16[64,1280]{1,0:T(8,128)(2,1)}), bf16[1024,1280]{1,0:T(8,128)(2,1)}) %all-gather.2.cloned.1.call-update) | async-done | bytes 2621456 | tf_op jit(solution)/shard_map/all_gather | solution.py:52
  351.2 3.2 fusion.2
  354.4 14.3 %all-to-all-start.5 = ((bf16[32,32,256]{2,1,0:T(8,128)(2,1)}), bf16[32,32,256]{2,1,0:T(8,128)(2,1)S(1)}, u32[]{:S(2)}, u32[]{:S(2)}) async-start(bf16[32,32,256]{2,1,0:T(8,128)(2,1)} %bitcast.44), calls=%async_computation.5 | async-start | bytes 1048576 | tf_op jit(solution)/shard_map/all_to_all | solution.py:174
  369.6 32.6 %all-to-all-done.5 = bf16[32,32,256]{2,1,0:T(8,128)(2,1)S(1)} async-done(((bf16[32,32,256]{2,1,0:T(8,128)(2,1)}), bf16[32,32,256]{2,1,0:T(8,128)(2,1)S(1)}, u32[]{:S(2)}, u32[]{:S(2)}) %all-to-all-start.5) | async-done | bytes 524320 | tf_op jit(solution)/shard_map/all_to_all | solution.py:174
  402.2 1.9 gather_fusion.1
  (100 shorter events, 31.4 us)
Async XLA Ops:
  6.5 45.1 %copy-start = (bf16[2048,256]{1,0:T(8,128)(2,1)S(1)}, bf16[2048,256]{1,0:T(8,128)(2,1)}, u32[]{:S(2)}) copy-start(bf16[2048,256]{1,0:T(8,128)(2,1)} %param.23) | copy-start | bytes 3145732
  6.5 28.1 %copy-start.4 = (bf16[256,256]{1,0:T(8,128)(2,1)S(1)}, bf16[256,256]{1,0:T(8,128)(2,1)}, u32[]{:S(2)}) copy-start(bf16[256,256]{1,0:T(8,128)(2,1)} %param.24) | copy-start | bytes 393220
  6.5 56.0 %copy-start.7 = (f32[256]{0:T(256)S(1)}, f32[256]{0:T(256)}, u32[]{:S(2)}) copy-start(f32[256]{0:T(256)} %param.25) | copy-start | bytes 3076
  7.6 8.8 %collective-permute-start = (bf16[30,128]{1,0:T(8,128)(2,1)S(1)}, bf16[30,128]{1,0:T(8,128)(2,1)S(1)}, u32[]{:S(2)}, u32[]{:S(2)}) collective-permute-start(bf16[30,128]{1,0:T(8,128)(2,1)S(1)} %slice.272), channel_id=1, source_target_pairs={{0,16},{16,32},{32,48},{48,64},{64,80},{80,96},{96,112},{112,128},... | collective-permute-start | bytes 23048 | tf_op jit(solution)/shard_map/ppermute | solution.py:15
  16.4 51.6 %copy-start.5 = (s32[256,2]{0,1:T(2,128)S(1)}, s32[256,2]{0,1:T(2,128)}, u32[]{:S(2)}) copy-start(s32[256,2]{0,1:T(2,128)} %param.26) | copy-start | bytes 6148
  30.9 20.7 %all-to-all-start.1 = ((bf16[16,256,128]{1,2,0:T(8,128)(2,1)}), bf16[16,256,128]{1,2,0:T(8,128)(2,1)S(1)}, u32[]{:S(2)}, u32[]{:S(2)}) async-start(bf16[16,256,128]{1,2,0:T(8,128)(2,1)} %broadcast_in_dim.25), calls=%async_computation.1 | async-start | bytes 2097152 | tf_op jit(solution)/shard_map/all_to_all | solution.py:20
  64.3 31.4 %all-to-all-start.3 = ((bf16[16,256,256]{2,1,0:T(8,128)(2,1)}), bf16[16,256,256]{2,1,0:T(8,128)(2,1)S(1)}, u32[]{:S(2)}, u32[]{:S(2)}) async-start(bf16[16,256,256]{2,1,0:T(8,128)(2,1)} %broadcast_in_dim.29), calls=%async_computation.3 | async-start | bytes 4194304 | tf_op jit(solution)/shard_map/all_to_all | solution.py:20
  95.7 1.3 copy-start.1
  109.1 53.1 %all-to-all-start.4 = ((bf16[32,2,4096]{2,1,0:T(2,128)(2,1)}), bf16[32,2,4096]{2,1,0:T(2,128)(2,1)}, u32[]{:S(2)}, u32[]{:S(2)}) async-start(bf16[32,2,4096]{2,1,0:T(2,128)(2,1)} %broadcast_select_fusion), calls=%async_computation.4 | async-start | bytes 1048576 | tf_op jit(solution)/shard_map/all_to_all | solution.py:159
  128.6 222.7 %all-gather.2.cloned.1.call-start = ((), (), s32[]{:S(2)}) async-start(), calls=%async_computation.6 | async-start | bytes 2785280 | tf_op jit(solution)/shard_map/all_gather | solution.py:52
  162.1 18.4 %collective-permute-start.1 = (bf16[32,2,4096]{2,1,0:T(2,128)(2,1)}, bf16[32,2,4096]{2,1,0:T(2,128)(2,1)S(1)}, u32[]{:S(2)}, u32[]{:S(2)}) collective-permute-start(bf16[32,2,4096]{2,1,0:T(2,128)(2,1)} %all-to-all-done.4), channel_id=1, source_target_pairs={{0,1},{1,2},{2,3},{3,4},{4,5},{5,6},{6,7},{7,8},{8,9},{9,10},{10,1... | collective-permute-start | bytes 1572872 | tf_op jit(solution)/shard_map/ppermute | solution.py:93
  164.1 18.4 %collective-permute-start.2 = (bf16[32,2,4096]{2,1,0:T(2,128)(2,1)}, bf16[32,2,4096]{2,1,0:T(2,128)(2,1)S(1)}, u32[]{:S(2)}, u32[]{:S(2)}) collective-permute-start(bf16[32,2,4096]{2,1,0:T(2,128)(2,1)} %all-to-all-done.4), channel_id=1, source_target_pairs={{0,15},{1,0},{2,1},{3,2},{4,3},{5,4},{6,5},{7,6},{8,7},{9,8},{10,9... | collective-permute-start | bytes 1572872 | tf_op jit(solution)/shard_map/ppermute | solution.py:98
  173.6 112.3 %copy-start.2 = (bf16[1,4096,64]{1,2,0:T(8,128)(2,1)S(1)}, bf16[1,4096,64]{1,2,0:T(8,128)(2,1)}, u32[]{:S(2)}) copy-start(bf16[1,4096,64]{1,2,0:T(8,128)(2,1)} %param.28) | copy-start | bytes 1572868
  180.5 17.3 %collective-permute-start.3 = (bf16[32,2,4096]{2,1,0:T(2,128)(2,1)S(1)}, bf16[32,2,4096]{2,1,0:T(2,128)(2,1)S(1)}, u32[]{:S(2)}, u32[]{:S(2)}) collective-permute-start(bf16[32,2,4096]{2,1,0:T(2,128)(2,1)S(1)} %collective-permute-done.1), channel_id=1, source_target_pairs={{0,1},{1,2},{2,3},{3,4},{4,5},{5,6},{6,7},{7,8},{8,9},{9,10},{10,1... | collective-permute-start | bytes 1572872 | tf_op jit(solution)/shard_map/ppermute | solution.py:93
  182.5 17.3 %collective-permute-start.4 = (bf16[32,2,4096]{2,1,0:T(2,128)(2,1)S(1)}, bf16[32,2,4096]{2,1,0:T(2,128)(2,1)S(1)}, u32[]{:S(2)}, u32[]{:S(2)}) collective-permute-start(bf16[32,2,4096]{2,1,0:T(2,128)(2,1)S(1)} %collective-permute-done.2), channel_id=1, source_target_pairs={{0,15},{1,0},{2,1},{3,2},{4,3},{5,4},{6,5},{7,6},{8,7},{9,8},{10,9... | collective-permute-start | bytes 1572872 | tf_op jit(solution)/shard_map/ppermute | solution.py:98
  197.9 16.5 %collective-permute-start.5 = (bf16[32,2,4096]{2,1,0:T(2,128)(2,1)S(1)}, bf16[32,2,4096]{2,1,0:T(2,128)(2,1)S(1)}, u32[]{:S(2)}, u32[]{:S(2)}) collective-permute-start(bf16[32,2,4096]{2,1,0:T(2,128)(2,1)S(1)} %collective-permute-done.3), channel_id=1, source_target_pairs={{0,1},{1,2},{2,3},{3,4},{4,5},{5,6},{6,7},{7,8},{8,9},{9,10},{10,1... | collective-permute-start | bytes 1572872 | tf_op jit(solution)/shard_map/ppermute | solution.py:93
  199.8 16.5 %collective-permute-start.6 = (bf16[32,2,4096]{2,1,0:T(2,128)(2,1)S(1)}, bf16[32,2,4096]{2,1,0:T(2,128)(2,1)S(1)}, u32[]{:S(2)}, u32[]{:S(2)}) collective-permute-start(bf16[32,2,4096]{2,1,0:T(2,128)(2,1)S(1)} %collective-permute-done.4), channel_id=1, source_target_pairs={{0,15},{1,0},{2,1},{3,2},{4,3},{5,4},{6,5},{7,6},{8,7},{9,8},{10,9... | collective-permute-start | bytes 1572872 | tf_op jit(solution)/shard_map/ppermute | solution.py:98
  214.3 15.6 %collective-permute-start.7 = (bf16[32,2,4096]{2,1,0:T(2,128)(2,1)S(1)}, bf16[32,2,4096]{2,1,0:T(2,128)(2,1)S(1)}, u32[]{:S(2)}, u32[]{:S(2)}) collective-permute-start(bf16[32,2,4096]{2,1,0:T(2,128)(2,1)S(1)} %collective-permute-done.5), channel_id=1, source_target_pairs={{0,1},{1,2},{2,3},{3,4},{4,5},{5,6},{6,7},{7,8},{8,9},{9,10},{10,1... | collective-permute-start | bytes 1572872 | tf_op jit(solution)/shard_map/ppermute | solution.py:93
  216.3 15.6 %collective-permute-start.8 = (bf16[32,2,4096]{2,1,0:T(2,128)(2,1)S(1)}, bf16[32,2,4096]{2,1,0:T(2,128)(2,1)S(1)}, u32[]{:S(2)}, u32[]{:S(2)}) collective-permute-start(bf16[32,2,4096]{2,1,0:T(2,128)(2,1)S(1)} %collective-permute-done.6), channel_id=1, source_target_pairs={{0,15},{1,0},{2,1},{3,2},{4,3},{5,4},{6,5},{7,6},{8,7},{9,8},{10,9... | collective-permute-start | bytes 1572872 | tf_op jit(solution)/shard_map/ppermute | solution.py:98
  229.9 14.8 %collective-permute-start.9 = (bf16[32,2,4096]{2,1,0:T(2,128)(2,1)S(1)}, bf16[32,2,4096]{2,1,0:T(2,128)(2,1)S(1)}, u32[]{:S(2)}, u32[]{:S(2)}) collective-permute-start(bf16[32,2,4096]{2,1,0:T(2,128)(2,1)S(1)} %collective-permute-done.7), channel_id=1, source_target_pairs={{0,1},{1,2},{2,3},{3,4},{4,5},{5,6},{6,7},{7,8},{8,9},{9,10},{10,1... | collective-permute-start | bytes 1572872 | tf_op jit(solution)/shard_map/ppermute | solution.py:93
  231.9 14.8 %collective-permute-start.10 = (bf16[32,2,4096]{2,1,0:T(2,128)(2,1)S(1)}, bf16[32,2,4096]{2,1,0:T(2,128)(2,1)S(1)}, u32[]{:S(2)}, u32[]{:S(2)}) collective-permute-start(bf16[32,2,4096]{2,1,0:T(2,128)(2,1)S(1)} %collective-permute-done.8), channel_id=1, source_target_pairs={{0,15},{1,0},{2,1},{3,2},{4,3},{5,4},{6,5},{7,6},{8,7},{9,8},{10,9... | collective-permute-start | bytes 1572872 | tf_op jit(solution)/shard_map/ppermute | solution.py:98
  244.7 13.9 %collective-permute-start.11 = (bf16[32,2,4096]{2,1,0:T(2,128)(2,1)S(1)}, bf16[32,2,4096]{2,1,0:T(2,128)(2,1)S(1)}, u32[]{:S(2)}, u32[]{:S(2)}) collective-permute-start(bf16[32,2,4096]{2,1,0:T(2,128)(2,1)S(1)} %collective-permute-done.9), channel_id=1, source_target_pairs={{0,1},{1,2},{2,3},{3,4},{4,5},{5,6},{6,7},{7,8},{8,9},{9,10},{10,1... | collective-permute-start | bytes 1572872 | tf_op jit(solution)/shard_map/ppermute | solution.py:93
  246.6 13.9 %collective-permute-start.12 = (bf16[32,2,4096]{2,1,0:T(2,128)(2,1)S(1)}, bf16[32,2,4096]{2,1,0:T(2,128)(2,1)S(1)}, u32[]{:S(2)}, u32[]{:S(2)}) collective-permute-start(bf16[32,2,4096]{2,1,0:T(2,128)(2,1)S(1)} %collective-permute-done.10), channel_id=1, source_target_pairs={{0,15},{1,0},{2,1},{3,2},{4,3},{5,4},{6,5},{7,6},{8,7},{9,8},{10,9... | collective-permute-start | bytes 1572872 | tf_op jit(solution)/shard_map/ppermute | solution.py:98
  254.1 34.4 %copy-start.8 = (bf16[1,4096,64]{1,2,0:T(8,128)(2,1)S(1)}, bf16[1,4096,64]{1,2,0:T(8,128)(2,1)}, u32[]{:S(2)}) copy-start(bf16[1,4096,64]{1,2,0:T(8,128)(2,1)} %param.29) | copy-start | bytes 1572868
  258.6 13.2 %collective-permute-start.13 = (bf16[32,2,4096]{2,1,0:T(2,128)(2,1)S(1)}, bf16[32,2,4096]{2,1,0:T(2,128)(2,1)S(1)}, u32[]{:S(2)}, u32[]{:S(2)}) collective-permute-start(bf16[32,2,4096]{2,1,0:T(2,128)(2,1)S(1)} %collective-permute-done.11), channel_id=1, source_target_pairs={{0,1},{1,2},{2,3},{3,4},{4,5},{5,6},{6,7},{7,8},{8,9},{9,10},{10,1... | collective-permute-start | bytes 1572872 | tf_op jit(solution)/shard_map/ppermute | solution.py:93
  260.5 14.2 %collective-permute-start.14 = (bf16[32,2,4096]{2,1,0:T(2,128)(2,1)S(1)}, bf16[32,2,4096]{2,1,0:T(2,128)(2,1)S(1)}, u32[]{:S(2)}, u32[]{:S(2)}) collective-permute-start(bf16[32,2,4096]{2,1,0:T(2,128)(2,1)S(1)} %collective-permute-done.12), channel_id=1, source_target_pairs={{0,15},{1,0},{2,1},{3,2},{4,3},{5,4},{6,5},{7,6},{8,7},{9,8},{10,9... | collective-permute-start | bytes 1572872 | tf_op jit(solution)/shard_map/ppermute | solution.py:98
  271.8 13.2 %collective-permute-start.15 = (bf16[32,2,4096]{2,1,0:T(2,128)(2,1)S(1)}, bf16[32,2,4096]{2,1,0:T(2,128)(2,1)S(1)}, u32[]{:S(2)}, u32[]{:S(2)}) collective-permute-start(bf16[32,2,4096]{2,1,0:T(2,128)(2,1)S(1)} %collective-permute-done.13), channel_id=1, source_target_pairs={{0,1},{1,2},{2,3},{3,4},{4,5},{5,6},{6,7},{7,8},{8,9},{9,10},{10,1... | collective-permute-start | bytes 1572872 | tf_op jit(solution)/shard_map/ppermute | solution.py:93
  285.9 65.4 %copy-start.9 = (bf16[1,1024,256]{2,1,0:T(8,128)(2,1)S(1)}, bf16[1,1024,256]{2,1,0:T(8,128)(2,1)}, u32[]{:S(2)}) copy-start(bf16[1,1024,256]{2,1,0:T(8,128)(2,1)} %param.30) | copy-start | bytes 1572868
  291.2 78.2 %copy-start.6 = (f32[256,2]{0,1:T(2,128)S(1)}, f32[256,2]{0,1:T(2,128)}, u32[]{:S(2)}) copy-start(f32[256,2]{0,1:T(2,128)} %param.27) | copy-start | bytes 6148
  291.3 114.7 %copy-start.3 = (bf16[1024,256]{1,0:T(8,128)(2,1)S(1)}, bf16[1024,256]{1,0:T(8,128)(2,1)}, u32[]{:S(2)}) copy-start(bf16[1024,256]{1,0:T(8,128)(2,1)} %param.33) | copy-start | bytes 1572868
  354.4 47.8 %all-to-all-start.5 = ((bf16[32,32,256]{2,1,0:T(8,128)(2,1)}), bf16[32,32,256]{2,1,0:T(8,128)(2,1)S(1)}, u32[]{:S(2)}, u32[]{:S(2)}) async-start(bf16[32,32,256]{2,1,0:T(8,128)(2,1)} %bitcast.44), calls=%async_computation.5 | async-start | bytes 1048576 | tf_op jit(solution)/shard_map/all_to_all | solution.py:174
Sparse Core Ops, SparseCore 0:
  292.1 59.1 all-gather.1
